TPU v7x, 128 devices: a whole 4x4x4 slice. The times are simulated.
128 devices in a mesh: sp: 16 (over z, x), dp: 8 (over y, core).
Axes of the slice: x: 4, y: 4, z: 4, core: 2. Of those that a mesh axis runs over, the one named last changes fastest.
Arguments:
- hidden_in: bfloat16 [8, 2048, 2048], P('dp', 'sp'), may hold values from -6 to 6
- in_weight: bfloat16 [2048, 512], P(('sp', 'dp')), may hold values from -0.125 to 0.125
- lam_real: float32 [32, 64], replicated, may hold values from -4 to 0, as said below
- lam_imag: float32 [32, 64], replicated, may hold values from 1 to 200
- log_step: float32 [32], replicated, may hold values from -4.61 to -2.3
- b_real: float32 [32, 64, 16], replicated, may hold values from -1 to 1
- b_imag: float32 [32, 64, 16], replicated, may hold values from -1 to 1
- c_real: float32 [32, 16, 64], replicated, may hold values from -0.3 to 0.3
- c_imag: float32 [32, 16, 64], replicated, may hold values from -0.3 to 0.3
- skip_weight: float32 [512], replicated, may hold values from -4 to 4
- lin_weight: bfloat16 [512, 2048], P(None, ('sp', 'dp')), may hold values from -0.25 to 0.25
- gate_weight: bfloat16 [512, 2048], P(None, ('sp', 'dp')), may hold values from -0.25 to 0.25
Outputs:
- mixed: bfloat16 [8, 2048, 2048], P('dp', 'sp')
Inputs may be any that keep to these rules, and one draw needn't show every extreme that they name: `lam_real`: negative in every entry.
All inputs are finite; a program needn't handle non-finite values.
Results may differ from a plain program's by a relative error of at most 0.0047.
The roundings to bfloat16 on the way count: a program that leaves them out, or rounds other values in their place, can miss the bound.
Values may be sent and summed in bfloat16 or wider, within the bound.
A program may use at most 64 MiB of HBM per device.

v0:
```python
import math
import jax
import jax.numpy as jnp
from jax import lax
from jax.sharding import PartitionSpec as P


def rows_first(arrays, axis, dims):
    turned = [jnp.moveaxis(a, dim, 0) for a, dim in zip(arrays, dims)]
    widths = [t[0].size for t in turned]
    both = jnp.concatenate([t.reshape(-1, w) for t, w in zip(turned, widths)], axis=1)
    out = lax.all_gather(both, axis, axis=0, tiled=True)
    tiles = jnp.split(out, [sum(widths[:k]) for k in range(1, len(widths))], axis=1)
    return tuple(
        (
            jnp.moveaxis(b.reshape(-1, *t.shape[1:]), 0, dim)
            for b, t, dim in zip(tiles, turned, dims)
        )
    )


def step_factors(lam_real, lam_imag, log_step, b_real, b_imag):
    step = jnp.exp(log_step)[:, None]
    xpart = lam_real * step
    wpart = lam_imag * step
    decay_re = jnp.exp(xpart) * jnp.cos(wpart)
    decay_im = jnp.exp(xpart) * jnp.sin(wpart)
    numer_re = jnp.expm1(xpart) * jnp.cos(wpart) - 2.0 * jnp.sin(0.5 * wpart) ** 2
    magnitude = lam_real * lam_real + lam_imag * lam_imag
    ratio_re = (numer_re * lam_real + decay_im * lam_imag) / magnitude
    ratio_im = (decay_im * lam_real - numer_re * lam_imag) / magnitude
    bbar_re = ratio_re[..., None] * b_real - ratio_im[..., None] * b_imag
    bbar_im = ratio_re[..., None] * b_imag + ratio_im[..., None] * b_real
    return (decay_re, decay_im, bbar_re, bbar_im)


def combine(left, right):
    lre, lim, lbre, lbim = left
    rre, rim, rbre, rbim = right
    return (
        rre * lre - rim * lim,
        rre * lim + rim * lre,
        rre * lbre - rim * lbim + rbre,
        rre * lbim + rim * lbre + rbim,
    )


def block_scan(piece, factors):
    decay_re, decay_im, bbar_re, bbar_im = factors
    highest = lax.Precision.HIGHEST
    block = piece.shape[0]
    groups_here, states = decay_re.shape
    lanes = groups_here * states
    source = piece.astype(jnp.float32)
    shaped = source.reshape(block, groups_here, source.shape[1] // groups_here)
    drive_re = jnp.einsum("tgh,gph->tgp", shaped, bbar_re, precision=highest).reshape(block, lanes)
    drive_im = jnp.einsum("tgh,gph->tgp", shaped, bbar_im, precision=highest).reshape(block, lanes)
    are = jnp.broadcast_to(decay_re.reshape(lanes), drive_re.shape)
    aim = jnp.broadcast_to(decay_im.reshape(lanes), drive_re.shape)
    return (source, lax.associative_scan(combine, (are, aim, drive_re, drive_im), axis=0))


def run_blocks(sequence, factors, out_re, out_im, direct, start):
    highest = lax.Precision.HIGHEST
    length, width = sequence.shape
    block = math.gcd(length, 512)
    blocks = sequence.reshape(length // block, block, width)
    groups_here, states = factors[0].shape

    def block_step(carry, piece):
        carry_re, carry_im = carry
        source, scanned = block_scan(piece, factors)
        cum_re, cum_im, local_re, local_im = scanned
        state_re = local_re + cum_re * carry_re - cum_im * carry_im
        state_im = local_im + cum_re * carry_im + cum_im * carry_re
        summed = jnp.einsum(
            "tgp,ghp->tgh", state_re.reshape(block, groups_here, states), out_re, precision=highest
        ) - jnp.einsum(
            "tgp,ghp->tgh", state_im.reshape(block, groups_here, states), out_im, precision=highest
        )
        result = jax.nn.gelu(summed.reshape(block, width) + direct * source)
        return ((state_re[-1], state_im[-1]), result.astype(jnp.bfloat16))

    _, results = lax.scan(block_step, start, blocks)
    return results.reshape(length, width)


def by_groups(sequence, lam_real, lam_imag, log_step, b_real, b_imag, c_real, c_imag, skip_weight):
    per_group = b_real.shape[2]
    groups_here = sequence.shape[1] // per_group
    first = lax.axis_index("sp") * groups_here
    pick = lambda table: lax.dynamic_slice_in_dim(table, first, groups_here, 0)
    factors = step_factors(
        pick(lam_real), pick(lam_imag), pick(log_step), pick(b_real), pick(b_imag)
    )
    direct = lax.dynamic_slice_in_dim(skip_weight, first * per_group, groups_here * per_group, 0)
    zeros = jnp.zeros((factors[0].size,), jnp.float32)
    return run_blocks(sequence, factors, pick(c_real), pick(c_imag), direct, (zeros, zeros))


def shards(
    hidden_in,
    in_weight,
    lam_real,
    lam_imag,
    log_step,
    b_real,
    b_imag,
    c_real,
    c_imag,
    skip_weight,
    lin_weight,
    gate_weight,
):
    tok_rows = hidden_in[0]
    whole_in, whole_lin, whole_gate = rows_first(
        (in_weight, lin_weight, gate_weight), ("sp", "dp"), (0, 1, 1)
    )
    inputs = jnp.dot(tok_rows, whole_in, preferred_element_type=jnp.float32).astype(jnp.bfloat16)
    sequence = lax.all_to_all(inputs, "sp", split_axis=1, concat_axis=0, tiled=True)
    mixer_local = by_groups(
        sequence, lam_real, lam_imag, log_step, b_real, b_imag, c_real, c_imag, skip_weight
    )
    mixer_out = lax.all_to_all(mixer_local, "sp", split_axis=0, concat_axis=1, tiled=True)
    linear = jnp.dot(mixer_out, whole_lin, preferred_element_type=jnp.float32)
    gate = jnp.dot(mixer_out, whole_gate, preferred_element_type=jnp.float32)
    mixed = (linear * jax.nn.sigmoid(gate)).astype(jnp.bfloat16)
    return mixed[None]


def solution(mesh):
    placed = (
        P("dp", "sp", None),
        P(("sp", "dp"), None),
        P(),
        P(),
        P(),
        P(),
        P(),
        P(),
        P(),
        P(),
        P(None, ("sp", "dp")),
        P(None, ("sp", "dp")),
    )
    return jax.shard_map(
        shards, mesh=mesh, in_specs=placed, out_specs=P("dp", "sp", None), check_vma=False
    )
```

profile of v0, /device:TPU:0, one launch (start us, length us, event | category | flops | bytes accessed | tf_op | source)
XLA Modules:
  0.0 268.4 jit_solution(9730837093817101557)
XLA Ops:
  6.5 1.4 pad_maximum_fusion.32
  8.0 0.7 dynamic-slice_exponential_fusion
  8.7 0.8 multiply_subtract_fusion.10
  9.8 0.8 add_divide_fusion
  11.3 0.7 multiply_add_fusion.9
  12.0 69.2 %all-gather.2.cloned.1.call-done = bf16[2048,1536]{1,0:T(8,128)(2,1)} async-done(((bf16[16,1536]{1,0:T(8,128)(2,1)}), bf16[2048,1536]{1,0:T(8,128)(2,1)}) %all-gather.2.cloned.1.call-update) | async-done | bytes 6291472 | tf_op jit(solution)/shard_map/all_gather | solution.py:12
  81.2 3.0 %fusion.18 = bf16[512,128]{1,0:T(8,128)(2,1)} fusion(bf16[2048,1536]{1,0:T(8,128)(2,1)} %all-gather.2.cloned.1.call-done, bf16[1,128,2048]{2,1,0:T(8,128)(2,1)S(1)} %copy-done), kind=kOutput, calls=%fused_computation.136 | convolution fusion | flops 268500992 | bytes 2752512 | tf_op jit(solution)/shard_map/dot_general | solution.py:119
  84.2 4.4 %all-to-all-start = ((bf16[128,16,32]{0,2,1:T(8,128)(2,1)}), bf16[128,16,32]{0,2,1:T(8,128)(2,1)S(1)}, u32[]{:S(2)}, u32[]{:S(2)}) async-start(bf16[128,16,32]{0,2,1:T(8,128)(2,1)} %bitcast.33), calls=%async_computation | async-start | bytes 262144 | tf_op jit(solution)/shard_map/all_to_all | solution.py:120
  89.5 1.3 dynamic_slice.38
  90.8 0.7 constant_dynamic-slice_fusion.1
  91.5 5.0 %all-to-all-done = bf16[128,16,32]{0,2,1:T(8,128)(2,1)S(1)} async-done(((bf16[128,16,32]{0,2,1:T(8,128)(2,1)}), bf16[128,16,32]{0,2,1:T(8,128)(2,1)S(1)}, u32[]{:S(2)}, u32[]{:S(2)}) %all-to-all-start) | async-done | bytes 131104 | tf_op jit(solution)/shard_map/all_to_all | solution.py:120
  97.8 146.7 %while.18 = (s32[]{:T(128)}, f32[128]{0:T(128)}, f32[128]{0:T(128)}, bf16[4,512,32]{1,2,0:T(8,128)(2,1)S(1)}, bf16[4,512,32]{1,2,0:T(8,128)(2,1)S(1)}, /*index=5...) while((s32[]{:T(128)}, f32[128]{0:T(128)}, ...), condition=%wide.wide.region_1.2_spmd, body=%wide.wide.region_0.1_spmd.sunk | while | flops 53527552 | bytes 26572484 | solution.py:84
  98.9 4.5 %slice.1651 = f32[255,128]{0,1:T(8,128)S(1)} slice(f32[512,128]{0,1:T(8,128)S(1)} %bitcast.197), slice={[2:512:2], [0:128:1]} | slice | bytes 261120 | tf_op jit(solution)/shard_map/while/body/eval_jaxpr/slice | solution.py:60
  103.5 4.5 %slice.1598 = f32[256,128]{0,1:T(8,128)S(1)} slice(f32[512,128]{0,1:T(8,128)S(1)} %bitcast.198), slice={[1:512:2], [0:128:1]} | slice | bytes 262144 | tf_op jit(solution)/shard_map/while/body/eval_jaxpr/slice | solution.py:60
  108.0 4.5 %slice.1596 = f32[256,128]{0,1:T(8,128)S(1)} slice(f32[512,128]{0,1:T(8,128)S(1)} %bitcast.199), slice={[0:511:2], [0:128:1]} | slice | bytes 262144 | tf_op jit(solution)/shard_map/while/body/eval_jaxpr/slice | solution.py:60
  113.2 4.5 %slice.1597 = f32[256,128]{0,1:T(8,128)S(1)} slice(f32[512,128]{0,1:T(8,128)S(1)} %bitcast.193), slice={[0:511:2], [0:128:1]} | slice | bytes 262144 | tf_op jit(solution)/shard_map/while/body/eval_jaxpr/slice | solution.py:60
  117.8 4.5 %slice.1595 = f32[256,128]{0,1:T(8,128)S(1)} slice(f32[512,128]{0,1:T(8,128)S(1)} %bitcast.194), slice={[1:512:2], [0:128:1]} | slice | bytes 262144 | tf_op jit(solution)/shard_map/while/body/eval_jaxpr/slice | solution.py:60
  122.3 4.5 %slice.1594 = f32[255,128]{0,1:T(8,128)S(1)} slice(f32[512,128]{0,1:T(8,128)S(1)} %bitcast.195), slice={[2:512:2], [0:128:1]} | slice | bytes 261120 | tf_op jit(solution)/shard_map/while/body/eval_jaxpr/slice | solution.py:60
  130.1 0.6 pad_maximum_fusion.126
  131.0 0.8 multiply_add_fusion.31
  133.7 0.8 fusion.70
  135.6 4.5 %slice.1651 = f32[255,128]{0,1:T(8,128)S(1)} slice(f32[512,128]{0,1:T(8,128)S(1)} %bitcast.197), slice={[2:512:2], [0:128:1]} | slice | bytes 261120 | tf_op jit(solution)/shard_map/while/body/eval_jaxpr/slice | solution.py:60
  140.2 4.5 %slice.1598 = f32[256,128]{0,1:T(8,128)S(1)} slice(f32[512,128]{0,1:T(8,128)S(1)} %bitcast.198), slice={[1:512:2], [0:128:1]} | slice | bytes 262144 | tf_op jit(solution)/shard_map/while/body/eval_jaxpr/slice | solution.py:60
  144.7 4.5 %slice.1596 = f32[256,128]{0,1:T(8,128)S(1)} slice(f32[512,128]{0,1:T(8,128)S(1)} %bitcast.199), slice={[0:511:2], [0:128:1]} | slice | bytes 262144 | tf_op jit(solution)/shard_map/while/body/eval_jaxpr/slice | solution.py:60
  149.9 4.5 %slice.1597 = f32[256,128]{0,1:T(8,128)S(1)} slice(f32[512,128]{0,1:T(8,128)S(1)} %bitcast.193), slice={[0:511:2], [0:128:1]} | slice | bytes 262144 | tf_op jit(solution)/shard_map/while/body/eval_jaxpr/slice | solution.py:60
  154.5 4.5 %slice.1595 = f32[256,128]{0,1:T(8,128)S(1)} slice(f32[512,128]{0,1:T(8,128)S(1)} %bitcast.194), slice={[1:512:2], [0:128:1]} | slice | bytes 262144 | tf_op jit(solution)/shard_map/while/body/eval_jaxpr/slice | solution.py:60
  159.0 4.5 %slice.1594 = f32[255,128]{0,1:T(8,128)S(1)} slice(f32[512,128]{0,1:T(8,128)S(1)} %bitcast.195), slice={[2:512:2], [0:128:1]} | slice | bytes 261120 | tf_op jit(solution)/shard_map/while/body/eval_jaxpr/slice | solution.py:60
  167.7 0.8 multiply_add_fusion.31
  170.3 0.8 fusion.70
  172.3 4.5 %slice.1651 = f32[255,128]{0,1:T(8,128)S(1)} slice(f32[512,128]{0,1:T(8,128)S(1)} %bitcast.197), slice={[2:512:2], [0:128:1]} | slice | bytes 261120 | tf_op jit(solution)/shard_map/while/body/eval_jaxpr/slice | solution.py:60
  176.9 4.5 %slice.1598 = f32[256,128]{0,1:T(8,128)S(1)} slice(f32[512,128]{0,1:T(8,128)S(1)} %bitcast.198), slice={[1:512:2], [0:128:1]} | slice | bytes 262144 | tf_op jit(solution)/shard_map/while/body/eval_jaxpr/slice | solution.py:60
  181.4 4.5 %slice.1596 = f32[256,128]{0,1:T(8,128)S(1)} slice(f32[512,128]{0,1:T(8,128)S(1)} %bitcast.199), slice={[0:511:2], [0:128:1]} | slice | bytes 262144 | tf_op jit(solution)/shard_map/while/body/eval_jaxpr/slice | solution.py:60
  186.6 4.5 %slice.1597 = f32[256,128]{0,1:T(8,128)S(1)} slice(f32[512,128]{0,1:T(8,128)S(1)} %bitcast.193), slice={[0:511:2], [0:128:1]} | slice | bytes 262144 | tf_op jit(solution)/shard_map/while/body/eval_jaxpr/slice | solution.py:60
  191.2 4.5 %slice.1595 = f32[256,128]{0,1:T(8,128)S(1)} slice(f32[512,128]{0,1:T(8,128)S(1)} %bitcast.194), slice={[1:512:2], [0:128:1]} | slice | bytes 262144 | tf_op jit(solution)/shard_map/while/body/eval_jaxpr/slice | solution.py:60
  195.7 4.5 %slice.1594 = f32[255,128]{0,1:T(8,128)S(1)} slice(f32[512,128]{0,1:T(8,128)S(1)} %bitcast.195), slice={[2:512:2], [0:128:1]} | slice | bytes 261120 | tf_op jit(solution)/shard_map/while/body/eval_jaxpr/slice | solution.py:60
  204.4 0.8 multiply_add_fusion.31
  207.0 0.8 fusion.70
  209.0 4.5 %slice.1651 = f32[255,128]{0,1:T(8,128)S(1)} slice(f32[512,128]{0,1:T(8,128)S(1)} %bitcast.197), slice={[2:512:2], [0:128:1]} | slice | bytes 261120 | tf_op jit(solution)/shard_map/while/body/eval_jaxpr/slice | solution.py:60
  213.6 4.5 %slice.1598 = f32[256,128]{0,1:T(8,128)S(1)} slice(f32[512,128]{0,1:T(8,128)S(1)} %bitcast.198), slice={[1:512:2], [0:128:1]} | slice | bytes 262144 | tf_op jit(solution)/shard_map/while/body/eval_jaxpr/slice | solution.py:60
  218.1 4.5 %slice.1596 = f32[256,128]{0,1:T(8,128)S(1)} slice(f32[512,128]{0,1:T(8,128)S(1)} %bitcast.199), slice={[0:511:2], [0:128:1]} | slice | bytes 262144 | tf_op jit(solution)/shard_map/while/body/eval_jaxpr/slice | solution.py:60
  223.3 4.5 %slice.1597 = f32[256,128]{0,1:T(8,128)S(1)} slice(f32[512,128]{0,1:T(8,128)S(1)} %bitcast.193), slice={[0:511:2], [0:128:1]} | slice | bytes 262144 | tf_op jit(solution)/shard_map/while/body/eval_jaxpr/slice | solution.py:60
  227.8 4.5 %slice.1595 = f32[256,128]{0,1:T(8,128)S(1)} slice(f32[512,128]{0,1:T(8,128)S(1)} %bitcast.194), slice={[1:512:2], [0:128:1]} | slice | bytes 262144 | tf_op jit(solution)/shard_map/while/body/eval_jaxpr/slice | solution.py:60
  232.3 4.5 %slice.1594 = f32[255,128]{0,1:T(8,128)S(1)} slice(f32[512,128]{0,1:T(8,128)S(1)} %bitcast.195), slice={[2:512:2], [0:128:1]} | slice | bytes 261120 | tf_op jit(solution)/shard_map/while/body/eval_jaxpr/slice | solution.py:60
  241.1 0.8 multiply_add_fusion.31
  243.7 0.8 fusion.70
  244.7 11.1 %all_to_all.35 = bf16[16,128,32]{1,2,0:T(8,128)(2,1)S(1)} all-to-all(bf16[16,128,32]{1,2,0:T(8,128)(2,1)S(1)} %copy.44), channel_id=1, replica_groups=mesh['sp'=16,'dp'=8] {'sp'}, dimensions={0} | all-to-all | bytes 262144 | tf_op jit(solution)/shard_map/all_to_all | solution.py:124
  255.8 2.5 fusion.11
  258.3 3.2 %fusion.13 = bf16[1,128,2048]{2,1,0:T(8,128)(2,1)} fusion(f32[128,2048]{1,0:T(8,128)S(1)} %fusion.11, bf16[128,512]{0,1:T(8,128)(2,1)S(1)} %bitcast.207, bf16[2048,1536]{1,0:T(8,128)(2,1)} %all-gather.2.cloned.1.call-done), kind=kOutput, calls=%fused_computation.131 | convolution fusion | flops 268959744 | bytes 3801088 | tf_op jit(solution)/shard_map/dot_general | solution.py:125
  (904 shorter events, 30.2 us)
Async XLA Ops:
  6.5 74.7 %copy-start = (bf16[1,128,2048]{2,1,0:T(8,128)(2,1)S(1)}, bf16[1,128,2048]{2,1,0:T(8,128)(2,1)}, u32[]{:S(2)}) copy-start(bf16[1,128,2048]{2,1,0:T(8,128)(2,1)} %param.14) | copy-start | bytes 1572868
  6.5 74.7 %all-gather.2.cloned.1.call-start = ((), (), s32[]{:S(2)}) async-start(), calls=%async_computation.2 | async-start | bytes 6340608 | tf_op jit(solution)/shard_map/all_gather | solution.py:12
  9.6 79.9 %copy-start.1 = (f32[2,64]{1,0:T(2,128)}, f32[2,64]{1,0:T(2,128)S(1)}, u32[]{:S(2)}) copy-start(f32[2,64]{1,0:T(2,128)S(1)} %get-tuple-element.1126) | copy-start | bytes 1540
  9.6 79.9 %copy-start.2 = (f32[2,64]{1,0:T(2,128)}, f32[2,64]{1,0:T(2,128)S(1)}, u32[]{:S(2)}) copy-start(f32[2,64]{1,0:T(2,128)S(1)} %get-tuple-element.1125) | copy-start | bytes 1540
  84.2 12.4 %all-to-all-start = ((bf16[128,16,32]{0,2,1:T(8,128)(2,1)}), bf16[128,16,32]{0,2,1:T(8,128)(2,1)S(1)}, u32[]{:S(2)}, u32[]{:S(2)}) async-start(bf16[128,16,32]{0,2,1:T(8,128)(2,1)} %bitcast.33), calls=%async_computation | async-start | bytes 262144 | tf_op jit(solution)/shard_map/all_to_all | solution.py:120
Sparse Core Ops, SparseCore 0:
  10.4 70.7 all-gather.1
where the time goes:
time: 269 us; the launch traced here: 268 us
  local copies, waits for them, and re-layouts  127 us (47%)
  waiting for transfers between devices  74.2 us (28%)
  other arithmetic  19.4 us (7%)
  between operations  13.5 us (5%)
  matrix products  13.3 us (5%)
  blocking collectives  11.1 us (4%)
  loops' own time  5.28 us (2%)
  starting transfers between devices  4.36 us (2%)
    slice x250, local copies, waits for them, and re-layouts, block_scan(): lax.associative_scan(combine, (are, aim, drive_re, drive_im), axis=0)  112 us
    all_gather x1, waiting for transfers between devices, rows_first(): out = lax.all_gather(both, axis, axis=0, tiled=True)  69.2 us
    all_to_all x1, blocking collectives, shards(): lax.all_to_all(mixer_local, 'sp', split_axis=0, concat_axis=1, tiled=True)  11.1 us
  transfers between devices with their start and end apart: 2, of which 2 were waited for; matrix products, arithmetic and copies ran while one was open for 3% of the time, Pallas kernels for 0%

commit v1 on v0

--- a/solution.py
+++ b/solution.py
@@ -9,7 +9,9 @@
     turned = [jnp.moveaxis(a, dim, 0) for a, dim in zip(arrays, dims)]
     widths = [t[0].size for t in turned]
     both = jnp.concatenate([t.reshape(-1, w) for t, w in zip(turned, widths)], axis=1)
-    out = lax.all_gather(both, axis, axis=0, tiled=True)
+    out = jnp.concatenate(
+        lax.all_to_all(jnp.stack([both] * lax.axis_size(axis)), axis, 0, 0), axis=0
+    )
     tiles = jnp.split(out, [sum(widths[:k]) for k in range(1, len(widths))], axis=1)
     return tuple(
         (

time: 269 us -> 393 us (1.46)
  other arithmetic: 19.4 us -> 123 us
  local copies, waits for them, and re-layouts: 127 us -> 141 us
  between operations: 13.5 us -> 0.09 us
  starting transfers between devices: 4.36 us -> 15.6 us
  matrix products: 13.3 us -> 21.9 us
  waiting for transfers between devices: 74.2 us -> 69.6 us
    all_gather x1 -> x0, waiting for transfers between devices: 69.2 us -> none  [rows_first(): out = lax.all_gather(both, axis, axis=0, tiled=True)]
    all_to_all x0 -> x1, waiting for transfers between devices: none -> 68 us  [rows_first(): lax.all_to_all(jnp.stack([both] * lax.axis_size(axis)), axis, 0, 0)]
    concatenate x128, other arithmetic: 3.75 us -> 42.4 us  [block_scan(): lax.associative_scan(combine, (are, aim, drive_re, drive_im), axis=0)]
    add x44, other arithmetic: 0.96 us -> 31.3 us  [combine(): rre * lbim + rim * lbre + rbim]
    add x26, other arithmetic: 0.38 us -> 18.1 us  [combine(): rre * lim + rim * lre]
    all_to_all x0 -> x1, starting transfers between devices: none -> 11.6 us  [rows_first(): lax.all_to_all(jnp.stack([both] * lax.axis_size(axis)), axis, 0, 0)]
    add x16, other arithmetic: 0.15 us -> 10.4 us  [combine(): rre * lbre - rim * lbim + rbre]
where the time goes in v1:
time: 393 us; the launch traced here: 389 us
  local copies, waits for them, and re-layouts  141 us (36%)
  other arithmetic  123 us (31%)
  waiting for transfers between devices  69.6 us (18%)
  matrix products  21.9 us (6%)
  starting transfers between devices  15.6 us (4%)
  blocking collectives  13.4 us (3%)
    slice x250, local copies, waits for them, and re-layouts, block_scan(): lax.associative_scan(combine, (are, aim, drive_re, drive_im), axis=0)  113 us
    all_to_all x1, waiting for transfers between devices, rows_first(): lax.all_to_all(jnp.stack([both] * lax.axis_size(axis)), axis, 0, 0)  68 us
    concatenate x128, other arithmetic, block_scan(): lax.associative_scan(combine, (are, aim, drive_re, drive_im), axis=0)  42.4 us
    add x44, other arithmetic, combine(): rre * lbim + rim * lbre + rbim  31.3 us
    add x26, other arithmetic, combine(): rre * lim + rim * lre  18.1 us
    all_to_all x1, blocking collectives, shards(): lax.all_to_all(mixer_local, 'sp', split_axis=0, concat_axis=1, tiled=True)  13.4 us
    all_to_all x1, starting transfers between devices, rows_first(): lax.all_to_all(jnp.stack([both] * lax.axis_size(axis)), axis, 0, 0)  11.6 us
    add x16, other arithmetic, combine(): rre * lbre - rim * lbim + rbre  10.4 us
  transfers between devices with their start and end apart: 2, of which 2 were waited for; matrix products, arithmetic and copies ran while one was open for 3% of the time, Pallas kernels for 0%

profile of v1, /device:TPU:0, one launch (start us, length us, event | category | flops | bytes accessed | tf_op | source)
XLA Modules:
  0.0 388.8 jit_solution(3769375787160031090)
XLA Ops:
  0.8 3.4 stack.2
  4.2 11.6 %all-to-all-start = ((bf16[128,16,1536]{2,1,0:T(8,128)(2,1)}), bf16[128,16,1536]{2,1,0:T(8,128)(2,1)}, u32[]{:S(2)}, u32[]{:S(2)}) async-start(bf16[128,16,1536]{2,1,0:T(8,128)(2,1)} %stack.2), calls=%async_computation | async-start | bytes 12582912 | tf_op jit(solution)/shard_map/all_to_all | solution.py:13
  20.2 1.3 add_multiply_fusion.9
  21.5 1.3 multiply_add_fusion.9
  22.9 68.0 %all-to-all-done = bf16[128,16,1536]{2,1,0:T(8,128)(2,1)} async-done(((bf16[128,16,1536]{2,1,0:T(8,128)(2,1)}), bf16[128,16,1536]{2,1,0:T(8,128)(2,1)}, u32[]{:S(2)}, u32[]{:S(2)}) %all-to-all-start) | async-done | bytes 6291488 | tf_op jit(solution)/shard_map/all_to_all | solution.py:13
  90.9 3.0 fusion.18
  93.9 4.0 %all-to-all-start.1 = ((bf16[128,16,32]{0,2,1:T(8,128)(2,1)}), bf16[128,16,32]{0,2,1:T(8,128)(2,1)S(1)}, u32[]{:S(2)}, u32[]{:S(2)}) async-start(bf16[128,16,32]{0,2,1:T(8,128)(2,1)} %bitcast.34), calls=%async_computation.1 | async-start | bytes 262144 | tf_op jit(solution)/shard_map/all_to_all | solution.py:122
  97.9 1.2 multiply_subtract_fusion.20
  101.6 1.3 dynamic_slice.38
  102.9 1.3 constant_dynamic-slice_fusion.1
  104.2 1.6 all-to-all-done.1
  107.8 260.8 %while.18 = (s32[]{:T(128)}, f32[128]{0:T(128)}, f32[128]{0:T(128)}, bf16[4,512,32]{1,2,0:T(8,128)(2,1)}, bf16[4,512,32]{1,2,0:T(8,128)(2,1)}, /*index=5*/f32[2,...) while((s32[]{:T(128)}, f32[128]{0:T(128)}, ...), condition=%wide.wide.region_1.2_spmd, body=%wide.wide.region_0.1_spmd.sunk | while | flops 53527552 | bytes 26573368 | solution.py:86
  108.8 4.5 %slice.1595 = f32[256,128]{0,1:T(8,128)S(1)} slice(f32[512,128]{0,1:T(8,128)S(1)} %bitcast.193), slice={[1:512:2], [0:128:1]} | slice | bytes 262144 | tf_op jit(solution)/shard_map/while/body/eval_jaxpr/slice | solution.py:62
  113.4 1.0 fusion.68
  114.5 4.5 %slice.1596 = f32[256,128]{0,1:T(8,128)S(1)} slice(f32[512,128]{0,1:T(8,128)S(1)} %bitcast.197), slice={[0:511:2], [0:128:1]} | slice | bytes 262144 | tf_op jit(solution)/shard_map/while/body/eval_jaxpr/slice | solution.py:62
  119.1 4.5 %slice.1597 = f32[256,128]{0,1:T(8,128)S(1)} slice(f32[512,128]{0,1:T(8,128)S(1)} %bitcast.194), slice={[0:511:2], [0:128:1]} | slice | bytes 262144 | tf_op jit(solution)/shard_map/while/body/eval_jaxpr/slice | solution.py:62
  123.7 4.5 %slice.1598 = f32[256,128]{0,1:T(8,128)S(1)} slice(f32[512,128]{0,1:T(8,128)S(1)} %bitcast.198), slice={[1:512:2], [0:128:1]} | slice | bytes 262144 | tf_op jit(solution)/shard_map/while/body/eval_jaxpr/slice | solution.py:62
  156.1 4.5 %slice.1594 = f32[255,128]{0,1:T(8,128)S(1)} slice(f32[512,128]{0,1:T(8,128)S(1)} %bitcast.195), slice={[2:512:2], [0:128:1]} | slice | bytes 261120 | tf_op jit(solution)/shard_map/while/body/eval_jaxpr/slice | solution.py:62
  160.7 4.5 %slice.1651 = f32[255,128]{0,1:T(8,128)S(1)} slice(f32[512,128]{0,1:T(8,128)S(1)} %bitcast.199), slice={[2:512:2], [0:128:1]} | slice | bytes 261120 | tf_op jit(solution)/shard_map/while/body/eval_jaxpr/slice | solution.py:62
  170.4 1.5 fusion.70
  174.0 4.5 %slice.1595 = f32[256,128]{0,1:T(8,128)S(1)} slice(f32[512,128]{0,1:T(8,128)S(1)} %bitcast.193), slice={[1:512:2], [0:128:1]} | slice | bytes 262144 | tf_op jit(solution)/shard_map/while/body/eval_jaxpr/slice | solution.py:62
  178.6 1.0 fusion.68
  179.7 4.5 %slice.1596 = f32[256,128]{0,1:T(8,128)S(1)} slice(f32[512,128]{0,1:T(8,128)S(1)} %bitcast.197), slice={[0:511:2], [0:128:1]} | slice | bytes 262144 | tf_op jit(solution)/shard_map/while/body/eval_jaxpr/slice | solution.py:62
  184.3 4.5 %slice.1597 = f32[256,128]{0,1:T(8,128)S(1)} slice(f32[512,128]{0,1:T(8,128)S(1)} %bitcast.194), slice={[0:511:2], [0:128:1]} | slice | bytes 262144 | tf_op jit(solution)/shard_map/while/body/eval_jaxpr/slice | solution.py:62
  188.9 4.5 %slice.1598 = f32[256,128]{0,1:T(8,128)S(1)} slice(f32[512,128]{0,1:T(8,128)S(1)} %bitcast.198), slice={[1:512:2], [0:128:1]} | slice | bytes 262144 | tf_op jit(solution)/shard_map/while/body/eval_jaxpr/slice | solution.py:62
  221.3 4.5 %slice.1594 = f32[255,128]{0,1:T(8,128)S(1)} slice(f32[512,128]{0,1:T(8,128)S(1)} %bitcast.195), slice={[2:512:2], [0:128:1]} | slice | bytes 261120 | tf_op jit(solution)/shard_map/while/body/eval_jaxpr/slice | solution.py:62
  225.9 4.5 %slice.1651 = f32[255,128]{0,1:T(8,128)S(1)} slice(f32[512,128]{0,1:T(8,128)S(1)} %bitcast.199), slice={[2:512:2], [0:128:1]} | slice | bytes 261120 | tf_op jit(solution)/shard_map/while/body/eval_jaxpr/slice | solution.py:62
  235.6 1.5 fusion.70
  239.2 4.5 %slice.1595 = f32[256,128]{0,1:T(8,128)S(1)} slice(f32[512,128]{0,1:T(8,128)S(1)} %bitcast.193), slice={[1:512:2], [0:128:1]} | slice | bytes 262144 | tf_op jit(solution)/shard_map/while/body/eval_jaxpr/slice | solution.py:62
  243.8 1.0 fusion.68
  244.9 4.5 %slice.1596 = f32[256,128]{0,1:T(8,128)S(1)} slice(f32[512,128]{0,1:T(8,128)S(1)} %bitcast.197), slice={[0:511:2], [0:128:1]} | slice | bytes 262144 | tf_op jit(solution)/shard_map/while/body/eval_jaxpr/slice | solution.py:62
  249.5 4.5 %slice.1597 = f32[256,128]{0,1:T(8,128)S(1)} slice(f32[512,128]{0,1:T(8,128)S(1)} %bitcast.194), slice={[0:511:2], [0:128:1]} | slice | bytes 262144 | tf_op jit(solution)/shard_map/while/body/eval_jaxpr/slice | solution.py:62
  254.1 4.5 %slice.1598 = f32[256,128]{0,1:T(8,128)S(1)} slice(f32[512,128]{0,1:T(8,128)S(1)} %bitcast.198), slice={[1:512:2], [0:128:1]} | slice | bytes 262144 | tf_op jit(solution)/shard_map/while/body/eval_jaxpr/slice | solution.py:62
  286.5 4.5 %slice.1594 = f32[255,128]{0,1:T(8,128)S(1)} slice(f32[512,128]{0,1:T(8,128)S(1)} %bitcast.195), slice={[2:512:2], [0:128:1]} | slice | bytes 261120 | tf_op jit(solution)/shard_map/while/body/eval_jaxpr/slice | solution.py:62
  291.1 4.5 %slice.1651 = f32[255,128]{0,1:T(8,128)S(1)} slice(f32[512,128]{0,1:T(8,128)S(1)} %bitcast.199), slice={[2:512:2], [0:128:1]} | slice | bytes 261120 | tf_op jit(solution)/shard_map/while/body/eval_jaxpr/slice | solution.py:62
  300.8 1.5 fusion.70
  304.4 4.5 %slice.1595 = f32[256,128]{0,1:T(8,128)S(1)} slice(f32[512,128]{0,1:T(8,128)S(1)} %bitcast.193), slice={[1:512:2], [0:128:1]} | slice | bytes 262144 | tf_op jit(solution)/shard_map/while/body/eval_jaxpr/slice | solution.py:62
  309.0 1.0 fusion.68
  310.1 4.5 %slice.1596 = f32[256,128]{0,1:T(8,128)S(1)} slice(f32[512,128]{0,1:T(8,128)S(1)} %bitcast.197), slice={[0:511:2], [0:128:1]} | slice | bytes 262144 | tf_op jit(solution)/shard_map/while/body/eval_jaxpr/slice | solution.py:62
  314.7 4.5 %slice.1597 = f32[256,128]{0,1:T(8,128)S(1)} slice(f32[512,128]{0,1:T(8,128)S(1)} %bitcast.194), slice={[0:511:2], [0:128:1]} | slice | bytes 262144 | tf_op jit(solution)/shard_map/while/body/eval_jaxpr/slice | solution.py:62
  319.3 4.5 %slice.1598 = f32[256,128]{0,1:T(8,128)S(1)} slice(f32[512,128]{0,1:T(8,128)S(1)} %bitcast.198), slice={[1:512:2], [0:128:1]} | slice | bytes 262144 | tf_op jit(solution)/shard_map/while/body/eval_jaxpr/slice | solution.py:62
  351.7 4.5 %slice.1594 = f32[255,128]{0,1:T(8,128)S(1)} slice(f32[512,128]{0,1:T(8,128)S(1)} %bitcast.195), slice={[2:512:2], [0:128:1]} | slice | bytes 261120 | tf_op jit(solution)/shard_map/while/body/eval_jaxpr/slice | solution.py:62
  356.3 4.5 %slice.1651 = f32[255,128]{0,1:T(8,128)S(1)} slice(f32[512,128]{0,1:T(8,128)S(1)} %bitcast.199), slice={[2:512:2], [0:128:1]} | slice | bytes 261120 | tf_op jit(solution)/shard_map/while/body/eval_jaxpr/slice | solution.py:62
  366.0 1.5 fusion.70
  368.5 1.0 copy.43
  369.7 13.4 %all_to_all.40 = bf16[16,128,32]{1,2,0:T(8,128)(2,1)S(1)} all-to-all(bf16[16,128,32]{1,2,0:T(8,128)(2,1)S(1)} %copy.44), channel_id=1, replica_groups=mesh['sp'=16,'dp'=8] {'sp'}, dimensions={0} | all-to-all | bytes 262144 | tf_op jit(solution)/shard_map/all_to_all | solution.py:126
  383.1 2.5 fusion.11
  385.5 3.2 fusion.13
  (906 shorter events, 148.9 us)
Async XLA Ops:
  0.0 90.9 %copy-start = (bf16[1,128,2048]{2,1,0:T(8,128)(2,1)S(1)}, bf16[1,128,2048]{2,1,0:T(8,128)(2,1)}, u32[]{:S(2)}) copy-start(bf16[1,128,2048]{2,1,0:T(8,128)(2,1)} %param.14) | copy-start | bytes 1572868
  4.2 11.7 %copy-start.3 = (f32[32]{0:T(128)S(1)}, f32[32]{0:T(128)}, u32[]{:S(2)}) copy-start(f32[32]{0:T(128)} %param.18) | copy-start | bytes 388
  4.2 86.7 %all-to-all-start = ((bf16[128,16,1536]{2,1,0:T(8,128)(2,1)}), bf16[128,16,1536]{2,1,0:T(8,128)(2,1)}, u32[]{:S(2)}, u32[]{:S(2)}) async-start(bf16[128,16,1536]{2,1,0:T(8,128)(2,1)} %stack.2), calls=%async_computation | async-start | bytes 12582912 | tf_op jit(solution)/shard_map/all_to_all | solution.py:13
  16.8 89.1 %copy-start.1 = (f32[2,64]{1,0:T(2,128)}, f32[2,64]{1,0:T(2,128)S(1)}, u32[]{:S(2)}) copy-start(f32[2,64]{1,0:T(2,128)S(1)} %get-tuple-element.1126) | copy-start | bytes 1540
  16.8 89.1 %copy-start.2 = (f32[2,64]{1,0:T(2,128)}, f32[2,64]{1,0:T(2,128)S(1)}, u32[]{:S(2)}) copy-start(f32[2,64]{1,0:T(2,128)S(1)} %get-tuple-element.1125) | copy-start | bytes 1540
  93.9 11.9 %all-to-all-start.1 = ((bf16[128,16,32]{0,2,1:T(8,128)(2,1)}), bf16[128,16,32]{0,2,1:T(8,128)(2,1)S(1)}, u32[]{:S(2)}, u32[]{:S(2)}) async-start(bf16[128,16,32]{0,2,1:T(8,128)(2,1)} %bitcast.34), calls=%async_computation.1 | async-start | bytes 262144 | tf_op jit(solution)/shard_map/all_to_all | solution.py:122
